TPU v7x, 32 devices: a whole 2x2x4 slice. The times are simulated.
32 devices in a mesh: sp: 8 (over z, x), tp: 4 (over y, core).
Axes of the slice: x: 2, y: 2, z: 4, core: 2. Of those that a mesh axis runs over, the one named last changes fastest.
Arguments:
- queries: bfloat16 [1536, 1536], P('sp', 'tp'), may hold values from -64 to 64
- latents: bfloat16 [1536, 512], P('sp'), may hold values from -6 to 6
- rope_key: bfloat16 [1536, 32], P('sp'), may hold values from -64 to 64
- w_key: bfloat16 [512, 1024], P(None, 'tp'), may hold values from -0.25 to 0.25
- w_value: bfloat16 [512, 1024], P(None, 'tp'), may hold values from -0.25 to 0.25
- w_out: bfloat16 [1024, 2048], P('tp'), may hold values from -0.59765625 to 0.59765625
- resid: bfloat16 [1536, 2048], P('sp', 'tp'), may hold values from -12 to 12
- gain_mix: float32 [2048], P('tp'), may hold values from 0.1 to 1.9
- w_gate: bfloat16 [2048, 3072], P('sp', 'tp'), may hold values from -0.125 to 0.125
- w_up: bfloat16 [2048, 3072], P('sp', 'tp'), may hold values from -0.125 to 0.125
- w_down: bfloat16 [3072, 2048], P('tp', 'sp'), may hold values from -0.41992188 to 0.41992188
- gain_out: float32 [2048], P('tp'), may hold values from 0.1 to 1.9
Outputs:
- layer_out: bfloat16 [1536, 2048], P('sp', 'tp')
All inputs are finite; a program needn't handle non-finite values.
Results may differ from a plain program's by a relative error of at most 0.014.
Values may be sent and summed in bfloat16 or wider, within the bound.
A program may use at most 128 MiB of HBM per device.

v0:
```python
import jax
import jax.numpy as jnp
from jax import lax
from jax.sharding import PartitionSpec as P

NOPE = 64
ROPE = 32
VDIM = 64
GRID_W = 64
ROTARY_BASE = 10000.0
NORM_EPSILON = 1e-06
DEEP_ALPHA = 8.0**0.25
HALF_STEP = 0.5


def rotary_tables(positions, rotary_width, grid_width):
    grid_rows = (positions // grid_width).astype(jnp.float32)
    grid_cols = (positions % grid_width).astype(jnp.float32)
    freq_count = rotary_width // 4
    inverse = ROTARY_BASE ** (-jnp.arange(freq_count, dtype=jnp.float32) / freq_count)
    angle_table = jnp.concatenate(
        [grid_rows[:, None] * inverse, grid_cols[:, None] * inverse], axis=-1
    )
    return (jnp.cos(angle_table), jnp.sin(angle_table))


def rotate(vectors, cosine, sine):
    half_width = vectors.shape[-1] // 2
    leading = vectors[..., :half_width].astype(jnp.float32)
    trailing = vectors[..., half_width:].astype(jnp.float32)
    return jnp.concatenate(
        [leading * cosine - trailing * sine, leading * sine + trailing * cosine], axis=-1
    ).astype(jnp.bfloat16)


def attend_block(state, key_block, query_pair):
    maxima, totals, running = state
    key_nope, value_rows, key_rope = key_block
    q_nope, q_rope = query_pair
    head_count = q_nope.shape[1]
    rows_here = key_nope.shape[0]
    key_nope = key_nope.reshape(rows_here, head_count, -1)
    value_rows = value_rows.reshape(rows_here, head_count, -1)
    score_scale = (q_nope.shape[2] + q_rope.shape[2]) ** (-0.5)
    scores = jnp.einsum("qhd,khd->hqk", q_nope, key_nope, preferred_element_type=jnp.float32)
    scores = (
        scores + jnp.einsum("qhd,kd->hqk", q_rope, key_rope, preferred_element_type=jnp.float32)
    ) * score_scale
    new_max = jnp.maximum(maxima, jnp.max(scores, axis=-1))
    weights = jnp.exp(scores - new_max[:, :, None])
    factor = jnp.exp(maxima - new_max)
    totals = totals * factor + jnp.sum(weights, axis=-1)
    update = jnp.einsum(
        "hqk,khd->qhd", weights.astype(jnp.bfloat16), value_rows, preferred_element_type=jnp.float32
    )
    running = running * jnp.transpose(factor)[:, :, None] + update
    return (new_max, totals, running)


def block_length(length):
    block_rows = length
    while block_rows > 2048 and block_rows % 2 == 0:
        block_rows = block_rows // 2
    return block_rows


def fold_keys(state, pieces, query_pair):
    length = pieces[0].shape[0]
    block_rows = block_length(length)
    if block_rows == length:
        return attend_block(state, pieces, query_pair)
    stacked = tuple(
        (member.reshape(length // block_rows, block_rows, member.shape[1]) for member in pieces)
    )

    def one_block(partial_value, key_block):
        return (attend_block(partial_value, key_block, query_pair), None)

    state, unused = lax.scan(one_block, state, stacked)
    return state


def split_norm(rows_in, gain_row):
    width_total = rows_in.shape[1] * lax.axis_size("tp")
    row_sums, squares = lax.psum(
        (jnp.sum(rows_in, axis=1), jnp.sum(rows_in * rows_in, axis=1)), "tp"
    )
    row_mean = row_sums / width_total
    variance = squares / width_total - row_mean * row_mean
    return (
        (rows_in - row_mean[:, None]) * lax.rsqrt(variance + NORM_EPSILON)[:, None] * gain_row
    ).astype(jnp.bfloat16)


def local(
    queries,
    latents,
    rope_key,
    w_key,
    w_value,
    w_out,
    resid,
    gain_mix,
    w_gate,
    w_up,
    w_down,
    gain_out,
):
    local_rows = queries.shape[0]
    head_count = w_key.shape[1] // NOPE
    offset = lax.axis_index("sp") * local_rows
    positions = offset + jnp.arange(local_rows, dtype=jnp.int32)
    cosine, sine = rotary_tables(positions, ROPE, GRID_W)
    key_rot = rotate(rope_key, cosine, sine)
    shaped = queries.reshape(local_rows, head_count, NOPE + ROPE)
    q_nope = shaped[:, :, :NOPE]
    q_rot = rotate(shaped[:, :, NOPE:], cosine[:, None, :], sine[:, None, :])
    query_pair = (q_nope, q_rot)
    start_state = (
        jnp.full((head_count, local_rows), -jnp.inf, jnp.float32),
        jnp.zeros((head_count, local_rows), jnp.float32),
        jnp.zeros((local_rows, head_count, VDIM), jnp.float32),
    )
    quarter = local_rows // lax.axis_size("tp")
    first_row = lax.axis_index("tp") * quarter
    latent_part = lax.dynamic_slice_in_dim(latents, first_row, quarter, 0)
    rotary_part = lax.dynamic_slice_in_dim(key_rot, first_row, quarter, 0)
    latent_all, rotary_all = (
        lax.all_gather(latent_part, "sp", axis=0, tiled=True),
        lax.all_gather(rotary_part, "sp", axis=0, tiled=True),
    )
    pieces = (
        lax.all_gather(latent_all, "tp", axis=0, tiled=True),
        lax.all_gather(rotary_all, "tp", axis=0, tiled=True),
    )
    key_nope = jnp.dot(pieces[0], w_key, preferred_element_type=jnp.float32).astype(jnp.bfloat16)
    value_rows = jnp.dot(pieces[0], w_value, preferred_element_type=jnp.float32).astype(
        jnp.bfloat16
    )
    state = fold_keys(start_state, (key_nope, value_rows, pieces[1]), query_pair)
    maxima, totals, running = state
    heads_out = (
        (running / jnp.transpose(totals)[:, :, None])
        .reshape(local_rows, head_count * VDIM)
        .astype(jnp.bfloat16)
    )
    projected = jnp.dot(heads_out, w_out, preferred_element_type=jnp.float32)
    attn_cols = lax.psum_scatter(
        projected.astype(jnp.bfloat16), "tp", scatter_dimension=1, tiled=True
    ).astype(jnp.float32)
    hidden_in = split_norm(DEEP_ALPHA * resid.astype(jnp.float32) + attn_cols, gain_mix)
    whole_rows = lax.all_gather(hidden_in, "tp", axis=1, tiled=True)
    pieces = (
        lax.all_gather(w_gate, "sp", axis=0, tiled=True),
        lax.all_gather(w_up, "sp", axis=0, tiled=True),
    )
    gate_sum = jnp.dot(whole_rows, pieces[0], preferred_element_type=jnp.float32)
    up_sum = jnp.dot(whole_rows, pieces[1], preferred_element_type=jnp.float32)
    hidden = (jax.nn.silu(gate_sum) * up_sum).astype(jnp.bfloat16)
    down_terms = jnp.dot(
        hidden, lax.all_gather(w_down, "sp", axis=1, tiled=True), preferred_element_type=jnp.float32
    )
    mixer_cols = lax.psum_scatter(
        down_terms.astype(jnp.bfloat16), "tp", scatter_dimension=1, tiled=True
    ).astype(jnp.float32)
    return split_norm(DEEP_ALPHA * hidden_in.astype(jnp.float32) + HALF_STEP * mixer_cols, gain_out)


def solution(mesh):
    placed = (
        P("sp", "tp"),
        P("sp", None),
        P("sp", None),
        P(None, "tp"),
        P(None, "tp"),
        P("tp", None),
        P("sp", "tp"),
        P("tp"),
        P("sp", "tp"),
        P("sp", "tp"),
        P("tp", "sp"),
        P("tp"),
    )
    return jax.shard_map(
        local, mesh=mesh, in_specs=placed, out_specs=P("sp", "tp"), check_vma=False
    )
```

profile of v0, /device:TPU:0, one launch (start us, length us, event | category | flops | bytes accessed | tf_op | source)
XLA Modules:
  0.0 324.2 jit_solution(2186468816205035295)
XLA Ops:
  7.4 0.9 constant_dynamic-slice_fusion
  8.3 34.8 %all_gather.24 = bf16[384,512]{1,0:T(8,128)(2,1)} all-gather(bf16[48,512]{1,0:T(8,128)(2,1)S(1)} %constant_dynamic-slice_fusion), channel_id=1, replica_groups=mesh['sp'=8,'tp'=4] {'sp'}, dimensions={0}, use_global_device_ids=true | all-gather | bytes 442368 | tf_op jit(solution)/shard_map/all_gather | solution.py:129
  43.3 0.8 fusion.40
  44.2 30.5 %all-gather = bf16[8,48,32]{1,2,0:T(8,128)(2,1)S(1)} all-gather(bf16[1,48,32]{1,2,0:T(8,128)(2,1)S(1)} %fusion.44), channel_id=1, replica_groups=mesh['sp'=8,'tp'=4] {'sp'}, dimensions={0}, use_global_device_ids=true | all-gather | bytes 27648 | tf_op jit(solution)/shard_map/all_gather | solution.py:130
  74.7 0.1 reshape.118
  74.9 1.0 copy.16
  75.9 5.3 %all_gather.27 = bf16[1536,32]{0,1:T(8,128)(2,1)S(1)} all-gather(bf16[384,32]{0,1:T(8,128)(2,1)S(1)} %reshape.118), channel_id=1, replica_groups=mesh['sp'=8,'tp'=4] {'tp'}, dimensions={0}, use_global_device_ids=true | all-gather | bytes 122880 | tf_op jit(solution)/shard_map/all_gather | solution.py:134
  81.3 2.9 fusion.28
  84.2 2.0 convolution_convert_fusion.1
  86.2 3.3 %fusion.50 = (f32[4,192]{1,0:T(4,128)S(1)}, f32[4,192,1536]{2,1,0:T(8,128)S(1)}) fusion(f32[1536,192,4]{0,1,2:T(8,128)} %fusion.28, bf16[1536,4,64]{0,2,1:T(8,128)(2,1)S(1)} %bitcast.45, bf16[192,4,96]{0,2,1:T(8,128)(2,1)S(1)} %bitcast.47), kind=kOutput, calls=%fused_computation.82 | convolution fusion | flops 154533120 | bytes 10357760 | tf_op jit(solution)/shard_map/qhd,khd->hqk/dot_general | solution.py:45
  89.6 0.8 fusion.1
  90.3 0.6 copy-done.1
  90.9 0.6 convolution_convert_fusion
  91.6 1.0 fusion.16
  92.6 1.3 convolution_convert_fusion.3
  94.0 0.5 all-gather.8.cloned.1.call-update
  94.6 0.5 all-gather.10.cloned.1.call-update
  95.1 0.5 all-gather.12.cloned.1.call-update
  95.7 22.5 %reduce-scatter.3.cloned.1.call-done = bf16[192,512]{1,0:T(8,128)(2,1)} async-done(((bf16[192,2048]{1,0:T(8,128)(2,1)}), bf16[192,512]{1,0:T(8,128)(2,1)}) %reduce-scatter.3.cloned.1.call-update) | async-done | bytes 196624 | tf_op jit(solution)/shard_map/reduce_scatter | solution.py:148
  118.3 1.1 fusion.24
  119.4 5.8 %all-reduce.1 = (f32[192]{0:T(256)S(1)}, f32[192]{0:T(256)S(1)}) all-reduce(f32[192]{0:T(256)S(1)} %get-tuple-element.8, f32[192]{0:T(256)S(1)} %get-tuple-element.7), channel_id=1, replica_groups=mesh['sp'=8,'tp'=4] {'tp'}, use_global_device_ids=true, to_apply=%region_6.7 | all-reduce | flops 384 | bytes 3072 | tf_op jit(solution)/shard_map/psum | solution.py:85
  125.2 1.1 multiply_convert_fusion.1
  126.2 8.3 %all_gather.28 = bf16[192,2048]{1,0:T(8,128)(2,1)S(1)} all-gather(bf16[192,512]{1,0:T(8,128)(2,1)S(1)} %multiply_convert_fusion.1), channel_id=1, replica_groups=mesh['sp'=8,'tp'=4] {'tp'}, dimensions={1}, use_global_device_ids=true | all-gather | bytes 983040 | tf_op jit(solution)/shard_map/all_gather | solution.py:152
  134.5 22.9 %all-gather.8.cloned.1.call-done = bf16[2048,768]{1,0:T(8,128)(2,1)} async-done(((bf16[256,768]{1,0:T(8,128)(2,1)}), bf16[2048,768]{1,0:T(8,128)(2,1)}) %all-gather.8.cloned.1.call-update) | async-done | bytes 3145744 | tf_op jit(solution)/shard_map/all_gather | solution.py:154
  157.5 2.7 fusion.51
  160.2 58.0 %all-gather.10.cloned.1.call-done = bf16[2048,768]{1,0:T(8,128)(2,1)} async-done(((bf16[256,768]{1,0:T(8,128)(2,1)}), bf16[2048,768]{1,0:T(8,128)(2,1)}) %all-gather.10.cloned.1.call-update) | async-done | bytes 3145744 | tf_op jit(solution)/shard_map/all_gather | solution.py:155
  218.1 63.1 %all-gather.12.cloned.1.call-done = bf16[768,2048]{1,0:T(8,128)(2,1)} async-done(((bf16[768,256]{1,0:T(8,128)(2,1)}), bf16[768,2048]{1,0:T(8,128)(2,1)}) %all-gather.12.cloned.1.call-update) | async-done | bytes 3145744 | tf_op jit(solution)/shard_map/all_gather | solution.py:161
  281.2 5.4 %convolution_convert_fusion.2 = bf16[192,2048]{1,0:T(8,128)(2,1)} fusion(bf16[768,2048]{1,0:T(8,128)(2,1)} %all-gather.12.cloned.1.call-done, bf16[192,2048]{1,0:T(8,128)(2,1)S(1)} %all_gather.28, bf16[2048,768]{1,0:T(8,128)(2,1)} %all-gather.10.cloned.1.call-done, f32[192,768]{1,0:T(8,128)S(1)} %fusion.51), kind=kOutput, calls=%fused_computation.7 | convolution fusion | flops 1209237504 | bytes 8454144 | tf_op jit(solution)/shard_map/dot_general | solution.py:160
  286.6 21.6 %reduce-scatter.5.cloned.1.call-done = bf16[192,512]{1,0:T(8,128)(2,1)} async-done(((bf16[192,2048]{1,0:T(8,128)(2,1)}), bf16[192,512]{1,0:T(8,128)(2,1)}) %reduce-scatter.5.cloned.1.call-update) | async-done | bytes 196624 | tf_op jit(solution)/shard_map/reduce_scatter | solution.py:163
  308.2 1.1 fusion.26
  309.3 5.8 %all-reduce = (f32[192]{0:T(256)S(1)}, f32[192]{0:T(256)S(1)}) all-reduce(f32[192]{0:T(256)S(1)} %get-tuple-element.6, f32[192]{0:T(256)S(1)} %get-tuple-element.5), channel_id=1, replica_groups=mesh['sp'=8,'tp'=4] {'tp'}, use_global_device_ids=true, to_apply=%region_11.12 | all-reduce | flops 384 | bytes 3072 | tf_op jit(solution)/shard_map/psum | solution.py:85
  315.1 1.7 multiply_convert_fusion
  (33 shorter events, 0.6 us)
Async XLA Ops:
  7.4 85.2 %copy-start = (bf16[256,2048]{1,0:T(8,128)(2,1)S(1)}, bf16[256,2048]{1,0:T(8,128)(2,1)}, u32[]{:S(2)}) copy-start(bf16[256,2048]{1,0:T(8,128)(2,1)} %param.17) | copy-start | bytes 3145732
  7.4 76.8 %all-gather.6.cloned.1.call-start = ((), (), s32[]{:S(2)}) async-start(), calls=%async_computation.2 | async-start | bytes 1966080 | tf_op jit(solution)/shard_map/all_gather | solution.py:133
  43.1 41.1 %copy-start.3 = (bf16[512,256]{1,0:T(8,128)(2,1)S(1)}, bf16[512,256]{1,0:T(8,128)(2,1)}, u32[]{:S(2)}) copy-start(bf16[512,256]{1,0:T(8,128)(2,1)} %param.15) | copy-start | bytes 786436
  43.1 75.1 %reduce-scatter.3.cloned.1.call-start = ((), (), s32[]{:S(2)}) async-start(), calls=%async_computation.3 | async-start | bytes 983040 | tf_op jit(solution)/shard_map/reduce_scatter | solution.py:148
  89.5 1.4 copy-start.1
  89.5 1.4 copy-start.4
  92.6 25.7 %copy-start.2 = (bf16[192,512]{1,0:T(8,128)(2,1)S(1)}, bf16[192,512]{1,0:T(8,128)(2,1)}, u32[]{:S(2)}) copy-start(bf16[192,512]{1,0:T(8,128)(2,1)} %param.18) | copy-start | bytes 589828
  92.6 32.6 %copy-start.5 = (f32[512]{0:T(512)S(1)}, f32[512]{0:T(512)}, u32[]{:S(2)}) copy-start(f32[512]{0:T(512)} %param.19) | copy-start | bytes 6148
  93.9 63.6 %all-gather.8.cloned.1.call-start = ((), (), s32[]{:S(2)}) async-start(), calls=%async_computation.4 | async-start | bytes 3538944 | tf_op jit(solution)/shard_map/all_gather | solution.py:154
  94.5 123.6 %all-gather.10.cloned.1.call-start = ((), (), s32[]{:S(2)}) async-start(), calls=%async_computation.5 | async-start | bytes 3538944 | tf_op jit(solution)/shard_map/all_gather | solution.py:155
  95.1 186.1 %all-gather.12.cloned.1.call-start = ((), (), s32[]{:S(2)}) async-start(), calls=%async_computation.6 | async-start | bytes 3538944 | tf_op jit(solution)/shard_map/all_gather | solution.py:161
  95.7 212.5 %reduce-scatter.5.cloned.1.call-start = ((), (), s32[]{:S(2)}) async-start(), calls=%async_computation.7 | async-start | bytes 983040 | tf_op jit(solution)/shard_map/reduce_scatter | solution.py:163
  160.2 154.9 %copy-start.6 = (f32[512]{0:T(512)S(1)}, f32[512]{0:T(512)}, u32[]{:S(2)}) copy-start(f32[512]{0:T(512)} %param.23) | copy-start | bytes 6148
Sparse Core Ops, SparseCore 0:
  43.3 20.5 all-gather.5
  94.0 24.1 reduce-scatter.2
  286.8 21.3 reduce-scatter.4
Sparse Core Ops, SparseCore 1:
  96.6 60.8 all-gather.7
  159.5 58.5 all-gather.9
  220.1 61.1 all-gather.11
where the time goes:
time: 325 us; the launch traced here: 324 us
  waiting for transfers between devices  190 us (58%)
  blocking collectives  90.5 us (28%)
  matrix products  19.2 us (6%)
  between operations  14.9 us (5%)
  other arithmetic  6.87 us (2%)
    all_gather x1, waiting for transfers between devices, local(): lax.all_gather(w_down, 'sp', axis=1, tiled=True)  63.1 us
    all_gather x1, waiting for transfers between devices, local(): lax.all_gather(w_up, 'sp', axis=0, tiled=True)  58 us
    all_gather x1, blocking collectives, local(): lax.all_gather(latent_part, 'sp', axis=0, tiled=True)  34.8 us
    all_gather x1, blocking collectives, local(): lax.all_gather(rotary_part, 'sp', axis=0, tiled=True)  30.5 us
    all_gather x1, waiting for transfers between devices, local(): lax.all_gather(w_gate, 'sp', axis=0, tiled=True)  22.9 us
    reduce_scatter x1, waiting for transfers between devices, local(): lax.psum_scatter(projected.astype(jnp.bfloat16), 'tp', scatter_dimension=...  22.5 us
    reduce_scatter x1, waiting for transfers between devices, local(): lax.psum_scatter(down_terms.astype(jnp.bfloat16), 'tp', scatter_dimension...  21.6 us
    psum x2, blocking collectives, split_norm(): lax.psum((jnp.sum(rows_in, axis=1), jnp.sum(rows_in * rows_in, axis=1)),...  11.5 us
  transfers between devices with their start and end apart: 6, of which 5 were waited for; matrix products, arithmetic and copies ran while one was open for 3% of the time, Pallas kernels for 0%

commit v1 on v0

--- a/solution.py
+++ b/solution.py
@@ -126,7 +126,9 @@
     latent_part = lax.dynamic_slice_in_dim(latents, first_row, quarter, 0)
     rotary_part = lax.dynamic_slice_in_dim(key_rot, first_row, quarter, 0)
     latent_all, rotary_all = (
-        lax.all_gather(latent_part, "sp", axis=0, tiled=True),
+        jnp.concatenate(
+            lax.all_to_all(jnp.stack([latent_part] * lax.axis_size("sp")), "sp", 0, 0), axis=0
+        ),
         lax.all_gather(rotary_part, "sp", axis=0, tiled=True),
     )
     pieces = (

time: 325 us -> 307 us (0.945)
  blocking collectives: 90.5 us -> 74.9 us
    all_gather x1 -> x0, blocking collectives: 34.8 us -> none  [local(): lax.all_gather(latent_part, 'sp', axis=0, tiled=True)]
    all_to_all x0 -> x1, blocking collectives: none -> 19.2 us  [local(): lax.all_to_all(jnp.stack([latent_part] * lax.axis_size('sp')), 'sp', 0, 0)]
where the time goes in v1:
time: 307 us; the launch traced here: 306 us
  waiting for transfers between devices  187 us (61%)
  blocking collectives  74.9 us (24%)
  matrix products  19.2 us (6%)
  between operations  14.9 us (5%)
  other arithmetic  6.87 us (2%)
    all_gather x1, waiting for transfers between devices, local(): lax.all_gather(w_down, 'sp', axis=1, tiled=True)  63.1 us
    all_gather x1, waiting for transfers between devices, local(): lax.all_gather(w_up, 'sp', axis=0, tiled=True)  58 us
    all_gather x1, blocking collectives, local(): lax.all_gather(rotary_part, 'sp', axis=0, tiled=True)  30.5 us
    all_gather x1, waiting for transfers between devices, local(): lax.all_gather(w_gate, 'sp', axis=0, tiled=True)  23 us
    reduce_scatter x1, waiting for transfers between devices, local(): lax.psum_scatter(down_terms.astype(jnp.bfloat16), 'tp', scatter_dimension...  21.6 us
    reduce_scatter x1, waiting for transfers between devices, local(): lax.psum_scatter(projected.astype(jnp.bfloat16), 'tp', scatter_dimension=...  20.3 us
    all_to_all x1, blocking collectives, local(): lax.all_to_all(jnp.stack([latent_part] * lax.axis_size('sp')), 'sp', 0, 0)  19.2 us
    psum x2, blocking collectives, split_norm(): lax.psum((jnp.sum(rows_in, axis=1), jnp.sum(rows_in * rows_in, axis=1)),...  11.5 us
  transfers between devices with their start and end apart: 6, of which 5 were waited for; matrix products, arithmetic and copies ran while one was open for 3% of the time, Pallas kernels for 0%

profile of v1, /device:TPU:0, one launch (start us, length us, event | category | flops | bytes accessed | tf_op | source)
XLA Modules:
  0.0 306.4 jit_solution(4426465764284885126)
XLA Ops:
  7.4 0.9 constant_dynamic-slice_fusion
  8.3 19.2 %all_to_all.5 = bf16[8,48,512]{2,1,0:T(8,128)(2,1)} all-to-all(bf16[8,48,512]{2,1,0:T(8,128)(2,1)S(1)} %stack.2), channel_id=1, replica_groups=mesh['sp'=8,'tp'=4] {'sp'}, dimensions={0} | all-to-all | bytes 786432 | tf_op jit(solution)/shard_map/all_to_all | solution.py:130
  27.7 0.8 fusion.40
  28.6 30.5 %all-gather = bf16[8,48,32]{1,2,0:T(8,128)(2,1)S(1)} all-gather(bf16[1,48,32]{1,2,0:T(8,128)(2,1)S(1)} %fusion.44), channel_id=1, replica_groups=mesh['sp'=8,'tp'=4] {'sp'}, dimensions={0}, use_global_device_ids=true | all-gather | bytes 27648 | tf_op jit(solution)/shard_map/all_gather | solution.py:132
  59.2 0.1 reshape.124
  59.3 1.0 copy.16
  60.3 5.3 %all_gather.23 = bf16[1536,32]{0,1:T(8,128)(2,1)S(1)} all-gather(bf16[384,32]{0,1:T(8,128)(2,1)S(1)} %reshape.124), channel_id=1, replica_groups=mesh['sp'=8,'tp'=4] {'tp'}, dimensions={0}, use_global_device_ids=true | all-gather | bytes 122880 | tf_op jit(solution)/shard_map/all_gather | solution.py:136
  65.7 2.9 fusion.28
  68.6 2.0 convolution_convert_fusion.1
  70.7 3.3 %fusion.50 = (f32[4,192]{1,0:T(4,128)S(1)}, f32[4,192,1536]{2,1,0:T(8,128)S(1)}) fusion(f32[1536,192,4]{0,1,2:T(8,128)} %fusion.28, bf16[1536,4,64]{0,2,1:T(8,128)(2,1)S(1)} %bitcast.46, bf16[192,4,96]{0,2,1:T(8,128)(2,1)S(1)} %bitcast.49), kind=kOutput, calls=%fused_computation.82 | convolution fusion | flops 154533120 | bytes 10357760 | tf_op jit(solution)/shard_map/qhd,khd->hqk/dot_general | solution.py:45
  74.0 0.8 fusion.1
  74.8 0.6 copy-done.1
  75.4 0.6 convolution_convert_fusion
  76.0 1.0 fusion.16
  77.0 1.3 convolution_convert_fusion.3
  78.4 0.5 all-gather.8.cloned.1.call-update
  79.0 0.5 all-gather.10.cloned.1.call-update
  79.6 0.5 all-gather.12.cloned.1.call-update
  80.1 20.3 %reduce-scatter.3.cloned.1.call-done = bf16[192,512]{1,0:T(8,128)(2,1)} async-done(((bf16[192,2048]{1,0:T(8,128)(2,1)}), bf16[192,512]{1,0:T(8,128)(2,1)}) %reduce-scatter.3.cloned.1.call-update) | async-done | bytes 196624 | tf_op jit(solution)/shard_map/reduce_scatter | solution.py:150
  100.4 1.1 fusion.24
  101.5 5.8 %all-reduce.1 = (f32[192]{0:T(256)S(1)}, f32[192]{0:T(256)S(1)}) all-reduce(f32[192]{0:T(256)S(1)} %get-tuple-element.8, f32[192]{0:T(256)S(1)} %get-tuple-element.7), channel_id=1, replica_groups=mesh['sp'=8,'tp'=4] {'tp'}, use_global_device_ids=true, to_apply=%region_6.7 | all-reduce | flops 384 | bytes 3072 | tf_op jit(solution)/shard_map/psum | solution.py:85
  107.3 1.1 multiply_convert_fusion.1
  108.4 8.3 %all_gather.24 = bf16[192,2048]{1,0:T(8,128)(2,1)S(1)} all-gather(bf16[192,512]{1,0:T(8,128)(2,1)S(1)} %multiply_convert_fusion.1), channel_id=1, replica_groups=mesh['sp'=8,'tp'=4] {'tp'}, dimensions={1}, use_global_device_ids=true | all-gather | bytes 983040 | tf_op jit(solution)/shard_map/all_gather | solution.py:154
  116.7 23.0 %all-gather.8.cloned.1.call-done = bf16[2048,768]{1,0:T(8,128)(2,1)} async-done(((bf16[256,768]{1,0:T(8,128)(2,1)}), bf16[2048,768]{1,0:T(8,128)(2,1)}) %all-gather.8.cloned.1.call-update) | async-done | bytes 3145744 | tf_op jit(solution)/shard_map/all_gather | solution.py:156
  139.7 2.7 fusion.51
  142.4 58.0 %all-gather.10.cloned.1.call-done = bf16[2048,768]{1,0:T(8,128)(2,1)} async-done(((bf16[256,768]{1,0:T(8,128)(2,1)}), bf16[2048,768]{1,0:T(8,128)(2,1)}) %all-gather.10.cloned.1.call-update) | async-done | bytes 3145744 | tf_op jit(solution)/shard_map/all_gather | solution.py:157
  200.3 63.1 %all-gather.12.cloned.1.call-done = bf16[768,2048]{1,0:T(8,128)(2,1)} async-done(((bf16[768,256]{1,0:T(8,128)(2,1)}), bf16[768,2048]{1,0:T(8,128)(2,1)}) %all-gather.12.cloned.1.call-update) | async-done | bytes 3145744 | tf_op jit(solution)/shard_map/all_gather | solution.py:163
  263.4 5.4 %convolution_convert_fusion.2 = bf16[192,2048]{1,0:T(8,128)(2,1)} fusion(bf16[768,2048]{1,0:T(8,128)(2,1)} %all-gather.12.cloned.1.call-done, bf16[192,2048]{1,0:T(8,128)(2,1)S(1)} %all_gather.24, bf16[2048,768]{1,0:T(8,128)(2,1)} %all-gather.10.cloned.1.call-done, f32[192,768]{1,0:T(8,128)S(1)} %fusion.51), kind=kOutput, calls=%fused_computation.7 | convolution fusion | flops 1209237504 | bytes 8454144 | tf_op jit(solution)/shard_map/dot_general | solution.py:162
  268.8 21.6 %reduce-scatter.5.cloned.1.call-done = bf16[192,512]{1,0:T(8,128)(2,1)} async-done(((bf16[192,2048]{1,0:T(8,128)(2,1)}), bf16[192,512]{1,0:T(8,128)(2,1)}) %reduce-scatter.5.cloned.1.call-update) | async-done | bytes 196624 | tf_op jit(solution)/shard_map/reduce_scatter | solution.py:165
  290.4 1.1 fusion.26
  291.5 5.8 %all-reduce = (f32[192]{0:T(256)S(1)}, f32[192]{0:T(256)S(1)}) all-reduce(f32[192]{0:T(256)S(1)} %get-tuple-element.6, f32[192]{0:T(256)S(1)} %get-tuple-element.5), channel_id=1, replica_groups=mesh['sp'=8,'tp'=4] {'tp'}, use_global_device_ids=true, to_apply=%region_11.12 | all-reduce | flops 384 | bytes 3072 | tf_op jit(solution)/shard_map/psum | solution.py:85
  297.3 1.7 multiply_convert_fusion
  (34 shorter events, 0.6 us)
Async XLA Ops:
  7.4 69.7 %copy-start = (bf16[256,2048]{1,0:T(8,128)(2,1)S(1)}, bf16[256,2048]{1,0:T(8,128)(2,1)}, u32[]{:S(2)}) copy-start(bf16[256,2048]{1,0:T(8,128)(2,1)} %param.17) | copy-start | bytes 3145732
  7.4 61.3 %all-gather.6.cloned.1.call-start = ((), (), s32[]{:S(2)}) async-start(), calls=%async_computation.3 | async-start | bytes 1966080 | tf_op jit(solution)/shard_map/all_gather | solution.py:135
  27.5 41.1 %copy-start.3 = (bf16[512,256]{1,0:T(8,128)(2,1)S(1)}, bf16[512,256]{1,0:T(8,128)(2,1)}, u32[]{:S(2)}) copy-start(bf16[512,256]{1,0:T(8,128)(2,1)} %param.15) | copy-start | bytes 786436
  27.6 72.9 %reduce-scatter.3.cloned.1.call-start = ((), (), s32[]{:S(2)}) async-start(), calls=%async_computation.4 | async-start | bytes 983040 | tf_op jit(solution)/shard_map/reduce_scatter | solution.py:150
  73.9 1.4 copy-start.1
  73.9 1.4 copy-start.4
  77.0 23.4 %copy-start.2 = (bf16[192,512]{1,0:T(8,128)(2,1)S(1)}, bf16[192,512]{1,0:T(8,128)(2,1)}, u32[]{:S(2)}) copy-start(bf16[192,512]{1,0:T(8,128)(2,1)} %param.18) | copy-start | bytes 589828
  77.0 30.3 %copy-start.5 = (f32[512]{0:T(512)S(1)}, f32[512]{0:T(512)}, u32[]{:S(2)}) copy-start(f32[512]{0:T(512)} %param.19) | copy-start | bytes 6148
  78.3 61.3 %all-gather.8.cloned.1.call-start = ((), (), s32[]{:S(2)}) async-start(), calls=%async_computation.5 | async-start | bytes 3538944 | tf_op jit(solution)/shard_map/all_gather | solution.py:156
  78.9 121.4 %all-gather.10.cloned.1.call-start = ((), (), s32[]{:S(2)}) async-start(), calls=%async_computation.6 | async-start | bytes 3538944 | tf_op jit(solution)/shard_map/all_gather | solution.py:157
  79.5 183.9 %all-gather.12.cloned.1.call-start = ((), (), s32[]{:S(2)}) async-start(), calls=%async_computation.7 | async-start | bytes 3538944 | tf_op jit(solution)/shard_map/all_gather | solution.py:163
  80.1 210.3 %reduce-scatter.5.cloned.1.call-start = ((), (), s32[]{:S(2)}) async-start(), calls=%async_computation.8 | async-start | bytes 983040 | tf_op jit(solution)/shard_map/reduce_scatter | solution.py:165
  142.3 154.9 %copy-start.6 = (f32[512]{0:T(512)S(1)}, f32[512]{0:T(512)}, u32[]{:S(2)}) copy-start(f32[512]{0:T(512)} %param.23) | copy-start | bytes 6148
Sparse Core Ops, SparseCore 0:
  27.7 18.3 all-gather.5
  78.5 21.9 reduce-scatter.2
  268.9 21.3 reduce-scatter.4
Sparse Core Ops, SparseCore 1:
  81.0 58.6 all-gather.7
  141.7 58.5 all-gather.9
  202.2 61.1 all-gather.11
